TPU v7x, 32 devices: a whole 2x2x4 slice. The times are simulated.
32 devices in a mesh: fs: 8 (over z, x), tp: 4 (over y, core).
Axes of the slice: x: 2, y: 2, z: 4, core: 2. Of those that a mesh axis runs over, the one named last changes fastest.
Arguments:
- tokens: bfloat16 [768, 4, 2048], P(None, 'tp'), may hold values from -6 to 6
- norm_gain: float32 [2048], P('fs'), may hold values from 0.1 to 1.9
- gate_weight: float32 [8, 2048, 4096], P(None, 'fs', 'tp'), may hold values from -0.125 to 0.125
- up_weight: float32 [8, 2048, 4096], P(None, 'fs', 'tp'), may hold values from -0.125 to 0.125
- down_weight: float32 [8, 2048, 4096], P(None, 'fs', 'tp'), may hold values from -0.09375 to 0.09375
- expert_ids: int32 [768, 4, 2], P(None, 'tp'), may hold values from 0 to 7, all different within a row
- expert_mix: float32 [768, 4, 2], P(None, 'tp'), may hold values from 0.2 to 1
Outputs:
- gate_serve: bfloat16 [8, 2048, 4096], P(None, None, 'fs')
- up_serve: bfloat16 [8, 2048, 4096], P(None, None, 'fs')
- down_serve: bfloat16 [8, 2048, 4096], P(None, None, 'fs')
- mixed: bfloat16 [768, 4, 2048], P('fs', 'tp')
Inputs may be any that keep to these rules, and one draw needn't show every extreme that they name: `expert_ids`: each token names two different experts.
All inputs are finite; a program needn't handle non-finite values.
Results may differ from a plain program's by a relative error of at most 0.0082.
Values may be sent and summed in bfloat16 or wider, within the bound.
A program may use at most 192 MiB of HBM per device.

v0:
```python
import jax
import jax.numpy as jnp
from jax import lax
from jax.sharding import PartitionSpec as P

norm_eps = 1e-05


def local(tokens, norm_gain, gate_weight, up_weight, down_weight, expert_ids, expert_mix):
    gate_folded = (gate_weight * norm_gain[None, :, None]).astype(jnp.bfloat16)
    up_folded = (up_weight * norm_gain[None, :, None]).astype(jnp.bfloat16)
    down_cast = down_weight.astype(jnp.bfloat16)
    regrouped = (
        lax.all_to_all(gate_folded, "tp", split_axis=0, concat_axis=2, tiled=True),
        lax.all_to_all(up_folded, "tp", split_axis=0, concat_axis=2, tiled=True),
        lax.all_to_all(down_cast, "tp", split_axis=0, concat_axis=2, tiled=True),
    )
    unit_split = (
        lax.all_to_all(regrouped[0], "fs", split_axis=2, concat_axis=1, tiled=True),
        lax.all_to_all(regrouped[1], "fs", split_axis=2, concat_axis=1, tiled=True),
        lax.all_to_all(regrouped[2], "fs", split_axis=2, concat_axis=1, tiled=True),
    )
    gate_serve, up_serve, down_serve = (
        lax.all_gather(unit_split[0], "tp", axis=0, tiled=True),
        lax.all_gather(unit_split[1], "tp", axis=0, tiled=True),
        lax.all_gather(unit_split[2], "tp", axis=0, tiled=True),
    )
    width = tokens.shape[2]
    token_rows = tokens.reshape(-1, width).astype(jnp.float32)
    row_mean = jnp.mean(token_rows, axis=1, keepdims=True)
    centered = token_rows - row_mean
    variance = jnp.mean(centered * centered, axis=1, keepdims=True)
    normed = (centered * lax.rsqrt(variance + norm_eps)).astype(jnp.bfloat16)
    route_ids = expert_ids.reshape(-1, 2)
    route_mix = expert_mix.reshape(-1, 2)
    expert_iota = jnp.arange(gate_serve.shape[0], dtype=jnp.int32)
    expert_gates = jnp.sum(
        (route_ids[:, :, None] == expert_iota[None, None, :]).astype(jnp.float32)
        * route_mix[:, :, None],
        axis=1,
    )
    gate_act = jnp.einsum("rd,edf->ref", normed, gate_serve, preferred_element_type=jnp.float32)
    up_act = jnp.einsum("rd,edf->ref", normed, up_serve, preferred_element_type=jnp.float32)
    hidden = (jax.nn.silu(gate_act) * up_act * expert_gates[:, :, None]).astype(jnp.bfloat16)
    own_rows = token_rows.shape[0] // lax.axis_size("fs")
    summed = lax.psum_scatter(
        jnp.einsum("ref,edf->rd", hidden, down_serve, preferred_element_type=jnp.float32),
        "fs",
        scatter_dimension=0,
        tiled=True,
    )
    mixed = summed.astype(jnp.bfloat16).reshape(own_rows, 1, width)
    return (gate_serve, up_serve, down_serve, mixed)


def solution(mesh):
    return jax.shard_map(
        local,
        mesh=mesh,
        in_specs=(
            P(None, "tp", None),
            P("fs"),
            P(None, "fs", "tp"),
            P(None, "fs", "tp"),
            P(None, "fs", "tp"),
            P(None, "tp", None),
            P(None, "tp", None),
        ),
        out_specs=(
            P(None, None, "fs"),
            P(None, None, "fs"),
            P(None, None, "fs"),
            P("fs", "tp", None),
        ),
        check_vma=False,
    )
```

profile of v0, /device:TPU:0, one launch (start us, length us, event | category | flops | bytes accessed | tf_op | source)
XLA Modules:
  0.0 917.8 jit_solution(5901348450162368212)
XLA Ops:
  7.2 0.0 all-gather.6.cloned.1.call-start
  7.2 12.0 %multiply_convert_fusion.1 = (bf16[8,256,1024]{2,1,0:T(8,128)(2,1)}, bf16[8,256,1024]{2,1,0:T(8,128)(2,1)}) fusion(f32[8,256,1024]{2,1,0:T(8,128)} %param.10, f32[256]{0:T(256)} %param.8, f32[8,256,1024]{2,1,0:T(8,128)} %param.9), kind=kLoop, calls=%fused_computation.2 | loop fusion | flops 8388608 | bytes 25166848 | tf_op jit(solution)/shard_map/convert_element_type | solution.py:11
  19.2 54.6 %all_to_all.108 = bf16[8,256,1024]{2,1,0:T(8,128)(2,1)} all-to-all(bf16[8,256,1024]{2,1,0:T(8,128)(2,1)} %get-tuple-element.4), channel_id=1, replica_groups=mesh['fs'=8,'tp'=4] {'tp'}, dimensions={0} | all-to-all | bytes 8388608 | tf_op jit(solution)/shard_map/all_to_all | solution.py:15
  73.7 6.2 copy.55
  80.0 8.4 copy.56
  88.4 99.4 %all_to_all.109 = bf16[2,256,4096]{1,0,2:T(2,128)(2,1)S(1)} all-to-all(bf16[2,256,4096]{1,0,2:T(2,128)(2,1)S(1)} %copy.56), channel_id=1, replica_groups=mesh['fs'=8,'tp'=4] {'fs'}, dimensions={2} | all-to-all | bytes 8388608 | tf_op jit(solution)/shard_map/all_to_all | solution.py:20
  187.8 2.6 copy.57
  190.3 6.2 copy.58
  196.5 0.0 all-gather.6.cloned.1.call-update
  196.5 0.0 all-gather.4.cloned.1.call-start
  196.6 96.1 %all_to_all.110 = bf16[8,256,1024]{2,1,0:T(8,128)(2,1)} all-to-all(bf16[8,256,1024]{2,1,0:T(8,128)(2,1)} %get-tuple-element.5), channel_id=1, replica_groups=mesh['fs'=8,'tp'=4] {'tp'}, dimensions={0} | all-to-all | bytes 8388608 | tf_op jit(solution)/shard_map/all_to_all | solution.py:14
  292.7 6.2 copy.51
  298.9 8.4 copy.52
  307.3 95.4 %all_to_all.111 = bf16[2,256,4096]{1,0,2:T(2,128)(2,1)S(1)} all-to-all(bf16[2,256,4096]{1,0,2:T(2,128)(2,1)S(1)} %copy.52), channel_id=1, replica_groups=mesh['fs'=8,'tp'=4] {'fs'}, dimensions={2} | all-to-all | bytes 8388608 | tf_op jit(solution)/shard_map/all_to_all | solution.py:19
  402.8 2.6 copy.53
  405.3 6.2 copy.54
  411.5 0.0 all-gather.4.cloned.1.call-update
  411.5 0.0 all-gather.8.cloned.1.call-start
  411.6 4.0 convert_element_type.27
  415.6 95.8 %all_to_all.112 = bf16[8,256,1024]{2,1,0:T(8,128)(2,1)} all-to-all(bf16[8,256,1024]{2,1,0:T(8,128)(2,1)S(1)} %convert_element_type.27), channel_id=1, replica_groups=mesh['fs'=8,'tp'=4] {'tp'}, dimensions={0} | all-to-all | bytes 8388608 | tf_op jit(solution)/shard_map/all_to_all | solution.py:16
  511.5 6.2 copy.59
  517.7 8.5 copy.60
  526.2 95.4 %all_to_all.113 = bf16[2,256,4096]{1,0,2:T(2,128)(2,1)S(1)} all-to-all(bf16[2,256,4096]{1,0,2:T(2,128)(2,1)S(1)} %copy.60), channel_id=1, replica_groups=mesh['fs'=8,'tp'=4] {'fs'}, dimensions={2} | all-to-all | bytes 8388608 | tf_op jit(solution)/shard_map/all_to_all | solution.py:21
  621.6 2.6 copy.61
  624.1 0.0 copy-start.1
  624.1 6.4 copy.62
  630.5 0.0 all-gather.8.cloned.1.call-update
  630.5 0.0 reduce-scatter.2.cloned.1.call-start
  630.6 0.0 copy-done.1
  630.6 0.0 copy-done.2
  630.6 0.0 copy-done
  630.6 0.5 convert_reduce_fusion
  631.1 1.0 fusion.4
  632.1 0.0 all-gather.6.cloned.1.call-done
  632.1 20.4 %fusion.11 = f32[768,8,512]{2,0,1:T(8,128)} fusion(bf16[8,2048,512]{2,1,0:T(8,128)(2,1)} %all-gather.6.cloned.1.call-done, bf16[768,1,2048]{2,0,1:T(8,128)(2,1)S(1)} %copy-done, f32[768]{0:T(1024)S(1)} %add_rsqrt_fusion, f32[768]{0:T(1024)S(1)} %broadcast_multiply_fusion), kind=kOutput, calls=%fused_computation.21 | convolution fusion | flops 12891193344 | bytes 32512000 | tf_op jit(solution)/shard_map/rd,edf->ref/dot_general | solution.py:43
  652.6 23.0 %multiply_convert_fusion.clone.6 = bf16[768,8,512]{2,0,1:T(8,128)(2,1)} fusion(f32[768,8,512]{2,0,1:T(8,128)} %fusion.11, bf16[8,2048,512]{2,1,0:T(8,128)(2,1)} %all-gather.4.cloned.1.call-done, f32[768,8]{0,1:T(8,128)S(1)} %select_reduce_fusion, bf16[768,1,2048]{2,0,1:T(8,128)(2,1)S(1)} %copy-done, f32[768]{0:T(1024)S(1)} %add_rsqrt_fusion, ...), kind=kOutput, calls=%fused_computation.clone.clone.clone.clone.clone.1 | convolution fusion | flops 12913213440 | bytes 38828032 | tf_op jit(solution)/shard_map/rd,edf->ref/dot_general | solution.py:42
  675.5 58.9 %all-gather.8.cloned.1.call-done = bf16[8,2048,512]{2,1,0:T(8,128)(2,1)} async-done(((bf16[2,2048,512]{2,1,0:T(8,128)(2,1)}), bf16[8,2048,512]{2,1,0:T(8,128)(2,1)}) %all-gather.8.cloned.1.call-update) | async-done | bytes 16777232 | tf_op jit(solution)/shard_map/all_gather | solution.py:26
  734.4 20.2 %fusion.8 = f32[768,2048]{1,0:T(8,128)} fusion(bf16[8,2048,512]{2,1,0:T(8,128)(2,1)} %all-gather.8.cloned.1.call-done, bf16[768,8,512]{2,0,1:T(8,128)(2,1)} %multiply_convert_fusion.clone.6), kind=kOutput, calls=%fused_computation.13 | convolution fusion | flops 12884901888 | bytes 29360128 | tf_op jit(solution)/shard_map/ref,edf->rd/dot_general | solution.py:47
  754.6 0.0 reduce-scatter.2.cloned.1.call-update
  754.7 118.2 %reduce-scatter.2.cloned.1.call-done = f32[96,2048]{1,0:T(8,128)} async-done(((f32[768,2048]{1,0:T(8,128)}), f32[96,2048]{1,0:T(8,128)}) %reduce-scatter.2.cloned.1.call-update) | async-done | bytes 786448 | tf_op jit(solution)/shard_map/reduce_scatter | solution.py:46
  872.8 1.9 convert_bitcast_fusion.1
  874.8 15.2 %copy.66 = bf16[8,2048,512]{2,1,0:T(8,128)(2,1)} copy(bf16[8,2048,512]{2,1,0:T(8,128)(2,1)} %all-gather.4.cloned.1.call-done) | data formatting | bytes 33554432
  889.9 15.2 %copy.67 = bf16[8,2048,512]{2,1,0:T(8,128)(2,1)} copy(bf16[8,2048,512]{2,1,0:T(8,128)(2,1)} %all-gather.6.cloned.1.call-done) | data formatting | bytes 33554432
  905.1 0.0 slice-done
  905.1 0.0 slice-done.1
  905.1 0.0 slice-done.2
  905.1 0.0 slice-done.3
  905.1 6.2 copy.68
  (11 shorter events, 0.0 us)
Async XLA Ops:
  7.2 625.0 %all-gather.6.cloned.1.call-start = ((), (), s32[]{:S(2)}) async-start(), calls=%async_computation.8 | async-start | bytes 20971520 | tf_op jit(solution)/shard_map/all_gather | solution.py:25
  196.5 456.0 %all-gather.4.cloned.1.call-start = ((), (), s32[]{:S(2)}) async-start(), calls=%async_computation.7 | async-start | bytes 20971520 | tf_op jit(solution)/shard_map/all_gather | solution.py:24
  411.5 322.9 %all-gather.8.cloned.1.call-start = ((), (), s32[]{:S(2)}) async-start(), calls=%async_computation.9 | async-start | bytes 20971520 | tf_op jit(solution)/shard_map/all_gather | solution.py:26
  624.1 6.5 copy-start.1
  624.1 6.5 copy-start.2
  624.1 6.5 copy-start
  630.5 242.3 %reduce-scatter.2.cloned.1.call-start = ((), (), s32[]{:S(2)}) async-start(), calls=%async_computation.10 | async-start | bytes 7077888 | tf_op jit(solution)/shard_map/reduce_scatter | solution.py:46
  874.8 30.3 %slice-start = ((s8[16777216]{0:T(1024)(128)(4,1)}), s8[4194304]{0:T(1024)(128)(4,1)S(1)}, s32[]{:S(2)}) async-start(s8[16777216]{0:T(1024)(128)(4,1)} %bitcast.67), calls=%async_computation.11 | async-start | bytes 8388608
  874.8 30.3 %slice-start.1 = ((s8[16777216]{0:T(1024)(128)(4,1)}), s8[4194304]{0:T(1024)(128)(4,1)S(1)}, s32[]{:S(2)}) async-start(s8[16777216]{0:T(1024)(128)(4,1)} %bitcast.67), calls=%async_computation.12 | async-start | bytes 8388608
  889.9 15.2 %slice-start.2 = ((s8[16777216]{0:T(1024)(128)(4,1)}), s8[4194304]{0:T(1024)(128)(4,1)S(1)}, s32[]{:S(2)}) async-start(s8[16777216]{0:T(1024)(128)(4,1)} %bitcast.67), calls=%async_computation.13 | async-start | bytes 8388608
  889.9 15.2 %slice-start.3 = ((s8[16777216]{0:T(1024)(128)(4,1)}), s8[4194304]{0:T(1024)(128)(4,1)S(1)}, s32[]{:S(2)}) async-start(s8[16777216]{0:T(1024)(128)(4,1)} %bitcast.67), calls=%async_computation.14 | async-start | bytes 8388608
Sparse Core Ops, SparseCore 0:
  196.7 145.7 all-gather.5
  411.7 147.4 all-gather.3
  630.7 103.7 all-gather.7
  754.8 117.9 reduce-scatter.1
where the time goes:
time: 919 us; the launch traced here: 918 us
  blocking collectives  537 us (58%)
  waiting for transfers between devices  177 us (19%)
  local copies, waits for them, and re-layouts  107 us (12%)
  matrix products  63.6 us (7%)
  other arithmetic  19.4 us (2%)
  between operations  13.9 us (2%)
    reduce_scatter x1, waiting for transfers between devices, local(): lax.psum_scatter(jnp.einsum('ref,edf->rd', hidden, down_serve, preferred_...  118 us
    all_to_all x1, blocking collectives, local(): lax.all_to_all(regrouped[1], 'fs', split_axis=2, concat_axis=1, tiled=True)  99.4 us
    all_to_all x1, blocking collectives, local(): lax.all_to_all(gate_folded, 'tp', split_axis=0, concat_axis=2, tiled=True)  96.1 us
    all_to_all x1, blocking collectives, local(): lax.all_to_all(down_cast, 'tp', split_axis=0, concat_axis=2, tiled=True)  95.8 us
    all_to_all x1, blocking collectives, local(): lax.all_to_all(regrouped[0], 'fs', split_axis=2, concat_axis=1, tiled=True)  95.4 us
    all_to_all x1, blocking collectives, local(): lax.all_to_all(regrouped[2], 'fs', split_axis=2, concat_axis=1, tiled=True)  95.4 us
    all_gather x1, waiting for transfers between devices, local(): lax.all_gather(unit_split[2], 'tp', axis=0, tiled=True)  58.9 us
    all_to_all x1, blocking collectives, local(): lax.all_to_all(up_folded, 'tp', split_axis=0, concat_axis=2, tiled=True)  54.6 us
  transfers between devices with their start and end apart: 4, of which 2 were waited for; matrix products, arithmetic and copies ran while one was open for 10% of the time, Pallas kernels for 0%

commit v1 on v0

v1 whole, which is shorter than its diff:
```python
import functools

import jax
import jax.numpy as jnp
from jax import lax
from jax.experimental import pallas as pl
from jax.experimental.pallas import tpu as pltpu
from jax.sharding import PartitionSpec as P

norm_eps = 1e-05
MESH = pl.DeviceIdType.MESH


def exchange_kernel(n_fs, n_tp, gate_in, up_in, down_in, gate_out, up_out, down_out, relay_buf,
                    hop_send, hop_recv, own_send, pass_send, core_send, side_send, land):
    ins, outs = (gate_in, up_in, down_in), (gate_out, up_out, down_out)
    experts, rows, columns = gate_in.shape
    per = n_fs // n_tp
    unit = columns // per
    f, t = lax.axis_index("fs"), lax.axis_index("tp")
    mate = t + 1 - 2 * lax.rem(t, 2)
    side = lax.rem(t + 2, n_tp)
    own = lax.div(f, per)
    own_mate = own + 1 - 2 * lax.rem(own, 2)
    near = t == own_mate
    far = t == lax.rem(own_mate + 2, n_tp)

    def hop(k, e):
        return pltpu.make_async_remote_copy(
            src_ref=ins[k].at[e], dst_ref=relay_buf.at[k - 1, e], send_sem=hop_send.at[k - 1, e],
            recv_sem=hop_recv.at[k - 1, e], device_id=(f, side), device_id_type=MESH)

    def straight(k, e, h):
        return pltpu.make_async_remote_copy(
            src_ref=ins[k].at[e, :, pl.ds(h * unit, unit)], dst_ref=outs[k].at[e, f], send_sem=own_send.at[k, e, h],
            recv_sem=land.at[k, e], device_id=(t * per + h, mate), device_id_type=MESH)

    def relayed(k, e, h):
        return pltpu.make_async_remote_copy(
            src_ref=relay_buf.at[k - 1, e, :, pl.ds(h * unit, unit)], dst_ref=outs[k].at[e, f],
            send_sem=pass_send.at[k - 1, e, h], recv_sem=land.at[k, e],
            device_id=(side * per + h, mate), device_id_type=MESH)

    def spread(k, e, to, sem):
        return pltpu.make_async_remote_copy(
            src_ref=outs[k].at[e], dst_ref=outs[k].at[e], send_sem=sem.at[k, e],
            recv_sem=land.at[k, e], device_id=(f, to), device_id_type=MESH)

    def to_mate(k, e):
        return spread(k, e, mate, core_send)

    def to_side(k, e):
        return spread(k, e, side, side_send)

    def landed(k, e):
        to_mate(k, e).wait_recv()

    def step(s, carry):
        @pl.when(s < experts)
        def _():
            hop(2, s).start()
            hop(1, s).start()
            for k in (0, 1):
                for h in range(per):
                    straight(k, s, h).start()

        @pl.when((s >= 1) & (s < experts + 1))
        def _():
            for k in (2, 1):
                hop(k, s - 1).wait_recv()
                for h in range(per):
                    relayed(k, s - 1, h).start()

        @pl.when((s >= 2) & (s < experts + 2))
        def _():
            e = s - 2

            @pl.when(near)
            def _():
                landed(0, e)
                to_side(0, e).start()
                to_mate(0, e).start()
                landed(1, e)
                to_mate(1, e).start()

            @pl.when(far)
            def _():
                landed(2, e)
                to_side(2, e).start()
                to_mate(2, e).start()
                landed(1, e)
                to_mate(1, e).start()

        @pl.when(s >= 3)
        def _():
            e = s - 3

            @pl.when(near)
            def _():
                landed(2, e)
                to_mate(2, e).start()

            @pl.when(far)
            def _():
                landed(0, e)
                to_mate(0, e).start()

        return carry

    lax.fori_loop(0, experts + 3, step, 0)

    def drain(e, carry):
        for k in (1, 2):
            hop(k, e).wait_send()
            for h in range(per):
                relayed(k, e, h).wait_send()
        for k in (0, 1):
            for h in range(per):
                straight(k, e, h).wait_send()

        @pl.when(near | far)
        def _():
            for k in range(3):
                to_mate(k, e).wait_send()

        @pl.when(near)
        def _():
            to_side(0, e).wait_send()

        @pl.when(far)
        def _():
            to_side(2, e).wait_send()

        @pl.when(jnp.logical_not(near | far))
        def _():
            for k in range(3):
                landed(k, e)

        return carry

    lax.fori_loop(0, experts, drain, 0)


def exchange(n_fs, n_tp, blocks):
    experts, rows, columns = blocks[0].shape
    per = n_fs // n_tp
    serve = jax.ShapeDtypeStruct((experts, n_fs, rows, columns // per), jnp.bfloat16)
    relay = jax.ShapeDtypeStruct((2, experts, rows, columns), jnp.bfloat16)
    dma = pltpu.SemaphoreType.DMA
    outs = pl.pallas_call(
        functools.partial(exchange_kernel, n_fs, n_tp),
        out_shape=(serve, serve, serve, relay),
        in_specs=[pl.BlockSpec(memory_space=pl.ANY)] * 3,
        out_specs=[pl.BlockSpec(memory_space=pl.ANY)] * 4,
        scratch_shapes=[
            dma((2, experts)),
            dma((2, experts)),
            dma((2, experts, per)),
            dma((2, experts, per)),
            dma((3, experts)),
            dma((3, experts)),
            dma((3, experts)),
        ],
        compiler_params=pltpu.CompilerParams(has_side_effects=True),
    )(*blocks)
    return tuple(out.reshape(experts, n_fs * rows, columns // per) for out in outs[:3])


def collective_exchange(blocks):
    regrouped = [lax.all_to_all(b, "tp", split_axis=0, concat_axis=2, tiled=True) for b in blocks]
    unit_split = [lax.all_to_all(b, "fs", split_axis=2, concat_axis=1, tiled=True) for b in regrouped]
    return tuple(lax.all_gather(b, "tp", axis=0, tiled=True) for b in unit_split)


def local(tokens, norm_gain, gate_weight, up_weight, down_weight, expert_ids, expert_mix):
    n_fs, n_tp = lax.axis_size("fs"), lax.axis_size("tp")
    blocks = (
        (gate_weight * norm_gain[None, :, None]).astype(jnp.bfloat16),
        (up_weight * norm_gain[None, :, None]).astype(jnp.bfloat16),
        down_weight.astype(jnp.bfloat16),
    )
    rows, columns = blocks[0].shape[1:]
    unit = columns * n_tp // n_fs
    if n_tp == 4 and n_fs % n_tp == 0 and unit % 128 == 0 and rows % 16 == 0:
        gate_serve, up_serve, down_serve = exchange(n_fs, n_tp, blocks)
    else:
        gate_serve, up_serve, down_serve = collective_exchange(blocks)
    width = tokens.shape[2]
    token_rows = tokens.reshape(-1, width).astype(jnp.float32)
    row_mean = jnp.mean(token_rows, axis=1, keepdims=True)
    centered = token_rows - row_mean
    variance = jnp.mean(centered * centered, axis=1, keepdims=True)
    normed = (centered * lax.rsqrt(variance + norm_eps)).astype(jnp.bfloat16)
    route_ids = expert_ids.reshape(-1, 2)
    route_mix = expert_mix.reshape(-1, 2)
    expert_iota = jnp.arange(gate_serve.shape[0], dtype=jnp.int32)
    expert_gates = jnp.sum(
        (route_ids[:, :, None] == expert_iota[None, None, :]).astype(jnp.float32)
        * route_mix[:, :, None],
        axis=1,
    )
    gate_act = jnp.einsum("rd,edf->ref", normed, gate_serve, preferred_element_type=jnp.float32)
    up_act = jnp.einsum("rd,edf->ref", normed, up_serve, preferred_element_type=jnp.float32)
    hidden = (jax.nn.silu(gate_act) * up_act * expert_gates[:, :, None]).astype(jnp.bfloat16)
    own_rows = token_rows.shape[0] // n_fs
    partial = jnp.einsum("ref,edf->rd", hidden, down_serve, preferred_element_type=jnp.float32)
    parts = partial.astype(jnp.bfloat16).reshape(n_fs, own_rows, width)
    parts = lax.all_to_all(parts, "fs", split_axis=0, concat_axis=0, tiled=True)
    summed = jnp.sum(parts.astype(jnp.float32), axis=0)
    mixed = summed.astype(jnp.bfloat16).reshape(own_rows, 1, width)
    return (gate_serve, up_serve, down_serve, mixed)


def solution(mesh):
    return jax.shard_map(
        local,
        mesh=mesh,
        in_specs=(
            P(None, "tp", None),
            P("fs"),
            P(None, "fs", "tp"),
            P(None, "fs", "tp"),
            P(None, "fs", "tp"),
            P(None, "tp", None),
            P(None, "tp", None),
        ),
        out_specs=(
            P(None, None, "fs"),
            P(None, None, "fs"),
            P(None, None, "fs"),
            P("fs", "tp", None),
        ),
        check_vma=False,
    )
```

time: 919 us -> 597 us (0.65)
  blocking collectives: 537 us -> 79 us
  Pallas kernels: 0 us -> 399 us
  waiting for transfers between devices: 177 us -> 0 us
  local copies, waits for them, and re-layouts: 107 us -> 36 us
  between operations: 13.9 us -> 0.72 us
    all_to_all x6 -> x1, blocking collectives: 537 us -> 79 us  [local(): parts = lax.all_to_all(parts, 'fs', split_axis=0, concat_axis=0, tiled=True)]
    pallas_call x0 -> x1, Pallas kernels: none -> 399 us  [exchange(): pl.pallas_call(functools.partial(exchange_kernel, n_fs, n_tp), out_shape=...]
    reduce_scatter x1 -> x0, waiting for transfers between devices: 118 us -> none  [local(): lax.psum_scatter(jnp.einsum('ref,edf->rd', hidden, down_serve, preferred_...]
    all_to_all x12 -> x0, local copies, waits for them, and re-layouts: 70.4 us -> none  [the longest x2 14.7 us: local(): lax.all_to_all(down_cast, 'tp', split_axis=0, concat_axis=2, tiled=True)]
    all_gather x3 -> x0, waiting for transfers between devices: 59 us -> none  [the longest x1 58.9 us: local(): lax.all_gather(unit_split[2], 'tp', axis=0, tiled=True)]
    unnamed x17 -> x19, local copies, waits for them, and re-layouts: 36.5 us -> 36 us
  transfers between devices with their start and end apart: 4 -> 0, of which waited for: 2 -> 0; matrix products, arithmetic and copies ran while one was open for 10% -> 0% of each run, Pallas kernels for 0% -> 0%
where the time goes in v1:
time: 597 us
  Pallas kernels  399 us (67%)
  blocking collectives  79 us (13%)
  matrix products  60.9 us (10%)
  local copies, waits for them, and re-layouts  36 us (6%)
  other arithmetic  21 us (4%)
    pallas_call x1, Pallas kernels, exchange(): pl.pallas_call(functools.partial(exchange_kernel, n_fs, n_tp), out_shape=...  399 us
    all_to_all x1, blocking collectives, local(): parts = lax.all_to_all(parts, 'fs', split_axis=0, concat_axis=0, tiled=True)  79 us
    unnamed x19, local copies, waits for them, and re-layouts  36 us
    dot_general x1, matrix products, local(): jnp.einsum('rd,edf->ref', normed, gate_serve, preferred_element_type=jnp....  22.8 us
    dot_general x1, matrix products, local(): jnp.einsum('rd,edf->ref', normed, up_serve, preferred_element_type=jnp.fl...  19.5 us
    dot_general x1, matrix products, local(): jnp.einsum('ref,edf->rd', hidden, down_serve, preferred_element_type=jnp....  18.6 us

profile of v1, /device:TPU:0, one launch (start us, length us, event | category | flops | bytes accessed | tf_op | source)
XLA Modules:
  0.0 597.0 jit_solution(12397624030139788898)
XLA Ops:
  0.6 0.0 copy-start
  0.6 6.2 %convert_element_type.35.down_in = bf16[8,256,1024]{2,1,0:T(8,128)(2,1)} convert(f32[8,256,1024]{2,1,0:T(8,128)} %param.11) | non-fusion elementwise | flops 2097152 | bytes 12582912 | tf_op jit(solution)/shard_map/convert_element_type | solution.py:180
  6.9 0.0 copy-done
  6.9 0.0 copy-start.3
  6.9 0.5 convert_reduce_fusion
  7.4 1.0 fusion.5
  8.3 0.0 copy-done.3
  8.3 11.9 %multiply_convert_fusion.1 = (bf16[8,256,1024]{2,1,0:T(8,128)(2,1)}, bf16[8,256,1024]{2,1,0:T(8,128)(2,1)}) fusion(f32[8,256,1024]{2,1,0:T(8,128)} %param.10, f32[256]{0:T(256)S(1)} %copy-done.3, f32[8,256,1024]{2,1,0:T(8,128)} %param.9), kind=kLoop, calls=%fused_computation.5 | loop fusion | flops 8388608 | bytes 25166848 | tf_op jit(solution)/shard_map/convert_element_type | solution.py:179
  20.2 399.4 %shard_map.102 = (bf16[8,8,256,512]{3,2,1,0:T(8,128)(2,1)}, bf16[8,8,256,512]{3,2,1,0:T(8,128)(2,1)}, bf16[8,8,256,512]{3,2,1,0:T(8,128)(2,1)}, bf16[2,8,256,1024]{3,2,1,0:T(8,128)(2,1)}) custom-call(bf16[8,256,1024]{2,1,0:T(8,128)(2,1)} %get-tuple-element.11.gate_in, bf16[8,256,1024]{2,1,0:T(8,128)(2,1)} %get-tuple-element.10.up_in, ...), custom_call_target="tpu_custom_call" | custom-call | tf_op jit(solution)/shard_map/pallas_call | solution.py:150
  419.6 0.0 copy-start.1
  419.6 0.0 copy-start.2
  419.6 19.5 %fusion.10 = f32[768,8,512]{2,0,1:T(8,128)} fusion(bf16[8,2048,512]{2,1,0:T(8,128)(2,1)} %bitcast.39, bf16[768,1,2048]{2,0,1:T(8,128)(2,1)S(1)} %copy-done, f32[768]{0:T(1024)S(1)} %add_rsqrt_fusion, f32[768]{0:T(1024)S(1)} %broadcast_multiply_fusion), kind=kOutput, calls=%fused_computation.21 | convolution fusion | flops 12891193344 | bytes 32512000 | tf_op jit(solution)/shard_map/rd,edf->ref/dot_general | solution.py:203
  439.2 0.0 copy-done.1
  439.2 0.0 copy-done.2
  439.2 22.8 %multiply_convert_fusion.clone.6 = bf16[768,8,512]{2,0,1:T(8,128)(2,1)} fusion(f32[768,8,512]{2,0,1:T(8,128)} %fusion.10, bf16[8,2048,512]{2,1,0:T(8,128)(2,1)} %bitcast.41, f32[768,8]{0,1:T(8,128)S(1)} %select_reduce_fusion, bf16[768,1,2048]{2,0,1:T(8,128)(2,1)S(1)} %copy-done, f32[768]{0:T(1024)S(1)} %add_rsqrt_fusion, ...), kind=kOutput, calls=%fused_computation.clone.clone.clone.clone.clone.1 | convolution fusion | flops 12913213440 | bytes 38828032 | tf_op jit(solution)/shard_map/rd,edf->ref/dot_general | solution.py:202
  462.0 18.6 %bitcast_convert_fusion = bf16[768,2048]{1,0:T(8,128)(2,1)S(1)} fusion(bf16[8,2048,512]{2,1,0:T(8,128)(2,1)} %bitcast.35, bf16[768,8,512]{2,0,1:T(8,128)(2,1)} %multiply_convert_fusion.clone.6), kind=kOutput, calls=%fused_computation.12 | convolution fusion | flops 12886474752 | bytes 26214400 | tf_op jit(solution)/shard_map/ref,edf->rd/dot_general | solution.py:206
  480.5 79.0 %all_to_all.5 = bf16[8,96,2048]{2,1,0:T(8,128)(2,1)S(1)} all-to-all(bf16[8,96,2048]{2,1,0:T(8,128)(2,1)S(1)} %bitcast.43), channel_id=1, replica_groups=mesh['fs'=8,'tp'=4] {'fs'}, dimensions={0} | all-to-all | bytes 6291456 | tf_op jit(solution)/shard_map/all_to_all | solution.py:208
  559.6 1.4 reduce_sum.42
  561.0 0.0 slice-start
  561.0 0.0 slice-start.1
  561.0 0.0 slice-start.2
  561.0 15.8 %copy.16 = bf16[8,2048,512]{2,1,0:T(8,128)(2,1)} copy(bf16[8,2048,512]{2,1,0:T(8,128)(2,1)} %bitcast.42) | data formatting | bytes 33554432
  576.8 0.0 slice-start.3
  576.8 14.0 %copy.17 = bf16[8,2048,512]{2,1,0:T(8,128)(2,1)} copy(bf16[8,2048,512]{2,1,0:T(8,128)(2,1)} %bitcast.40) | data formatting | bytes 33554432
  590.8 0.0 slice-done
  590.8 0.0 slice-done.1
  590.8 0.0 slice-done.2
  590.8 0.0 slice-done.3
  590.8 6.2 %copy.18 = bf16[8,2048,512]{2,1,0:T(8,128)(2,1)} copy(bf16[8,2048,512]{2,1,0:T(8,128)(2,1)S(1)} %bitcast.38) | data formatting | bytes 33554432
  (4 shorter events, 0.0 us)
Async XLA Ops:
  0.6 6.2 %copy-start = (bf16[768,1,2048]{2,0,1:T(8,128)(2,1)S(1)}, bf16[768,1,2048]{2,0,1:T(8,128)(2,1)}, u32[]{:S(2)}) copy-start(bf16[768,1,2048]{2,0,1:T(8,128)(2,1)} %param.7) | copy-start | bytes 9437188
  6.9 1.5 copy-start.3
  419.6 19.5 %copy-start.1 = (f32[768,1,2]{0,2,1:T(2,128)S(1)}, f32[768,1,2]{0,2,1:T(2,128)}, u32[]{:S(2)}) copy-start(f32[768,1,2]{0,2,1:T(2,128)} %param.13) | copy-start | bytes 18436
  419.6 19.5 %copy-start.2 = (s32[768,1,2]{0,2,1:T(2,128)S(1)}, s32[768,1,2]{0,2,1:T(2,128)}, u32[]{:S(2)}) copy-start(s32[768,1,2]{0,2,1:T(2,128)} %param.12) | copy-start | bytes 18436
  561.0 29.8 %slice-start = ((s8[16777216]{0:T(1024)(128)(4,1)}), s8[4194304]{0:T(1024)(128)(4,1)S(1)}, s32[]{:S(2)}) async-start(s8[16777216]{0:T(1024)(128)(4,1)} %bitcast.36), calls=%async_computation.1 | async-start | bytes 8388608
  561.0 29.8 %slice-start.1 = ((s8[16777216]{0:T(1024)(128)(4,1)}), s8[4194304]{0:T(1024)(128)(4,1)S(1)}, s32[]{:S(2)}) async-start(s8[16777216]{0:T(1024)(128)(4,1)} %bitcast.36), calls=%async_computation.2 | async-start | bytes 8388608
  561.0 29.8 %slice-start.2 = ((s8[16777216]{0:T(1024)(128)(4,1)}), s8[4194304]{0:T(1024)(128)(4,1)S(1)}, s32[]{:S(2)}) async-start(s8[16777216]{0:T(1024)(128)(4,1)} %bitcast.36), calls=%async_computation.3 | async-start | bytes 8388608
  576.8 14.0 %slice-start.3 = ((s8[16777216]{0:T(1024)(128)(4,1)}), s8[4194304]{0:T(1024)(128)(4,1)S(1)}, s32[]{:S(2)}) async-start(s8[16777216]{0:T(1024)(128)(4,1)} %bitcast.36), calls=%async_computation.4 | async-start | bytes 8388608

commit v2 on v1

--- a/solution.py
+++ b/solution.py
@@ -11,8 +11,8 @@
 MESH = pl.DeviceIdType.MESH
 
 
-def exchange_kernel(n_fs, n_tp, gate_in, up_in, down_in, gate_out, up_out, down_out, relay_buf,
-                    hop_send, hop_recv, own_send, pass_send, core_send, side_send, land):
+def exchange_kernel(n_fs, n_tp, gate_in, up_in, down_in, normed, gates, gate_out, up_out, down_out, relay_buf,
+                    partial, held, total, hop_send, hop_recv, own_send, pass_send, core_send, side_send, land, load):
     ins, outs = (gate_in, up_in, down_in), (gate_out, up_out, down_out)
     experts, rows, columns = gate_in.shape
     per = n_fs // n_tp
@@ -55,6 +55,31 @@
     def landed(k, e):
         to_mate(k, e).wait_recv()
 
+    tall = normed.shape[0] // 2
+    deep = n_fs * rows
+
+    def compute(e):
+        loads = [pltpu.make_async_copy(outs[k].at[e], held.at[k], load.at[k]) for k in range(3)]
+        for copy in loads:
+            copy.start()
+        for copy in loads:
+            copy.wait()
+
+        def some_rows(i, carry):
+            now = pl.ds(pl.multiple_of(i * tall, tall), tall)
+            tokens = normed[now, :]
+            gate_act = jnp.dot(tokens, held[0].reshape(deep, unit), preferred_element_type=jnp.float32)
+            up_act = jnp.dot(tokens, held[1].reshape(deep, unit), preferred_element_type=jnp.float32)
+            hidden = gate_act / (1.0 + jnp.exp(-gate_act)) * up_act * gates[e, now, :]
+            total[now, :] += lax.dot_general(
+                hidden.astype(jnp.bfloat16), held[2].reshape(deep, unit), (((1,), (1,)), ((), ())),
+                preferred_element_type=jnp.float32)
+            return carry
+
+        lax.fori_loop(0, 2, some_rows, 0)
+
+    total[...] = jnp.zeros_like(total)
+
     def step(s, carry):
         @pl.when(s < experts)
         def _():
@@ -105,9 +130,17 @@
                 landed(0, e)
                 to_mate(0, e).start()
 
+            @pl.when(jnp.logical_not(near | far))
+            def _():
+                for k in range(3):
+                    landed(k, e)
+
+            compute(e)
+
         return carry
 
     lax.fori_loop(0, experts + 3, step, 0)
+    partial[...] = total[...].astype(jnp.bfloat16)
 
     def drain(e, carry):
         for k in (1, 2):
@@ -131,17 +164,12 @@
         def _():
             to_side(2, e).wait_send()
 
-        @pl.when(jnp.logical_not(near | far))
-        def _():
-            for k in range(3):
-                landed(k, e)
-
         return carry
 
     lax.fori_loop(0, experts, drain, 0)
 
 
-def exchange(n_fs, n_tp, blocks):
+def exchange(n_fs, n_tp, blocks, normed, gates):
     experts, rows, columns = blocks[0].shape
     per = n_fs // n_tp
     serve = jax.ShapeDtypeStruct((experts, n_fs, rows, columns // per), jnp.bfloat16)
@@ -149,10 +177,12 @@
     dma = pltpu.SemaphoreType.DMA
     outs = pl.pallas_call(
         functools.partial(exchange_kernel, n_fs, n_tp),
-        out_shape=(serve, serve, serve, relay),
-        in_specs=[pl.BlockSpec(memory_space=pl.ANY)] * 3,
-        out_specs=[pl.BlockSpec(memory_space=pl.ANY)] * 4,
+        out_shape=(serve, serve, serve, relay, jax.ShapeDtypeStruct(normed.shape, jnp.bfloat16)),
+        in_specs=[pl.BlockSpec(memory_space=pl.ANY)] * 3 + [pl.BlockSpec(memory_space=pltpu.VMEM)] * 2,
+        out_specs=[pl.BlockSpec(memory_space=pl.ANY)] * 4 + [pl.BlockSpec(memory_space=pltpu.VMEM)],
         scratch_shapes=[
+            pltpu.VMEM((3, n_fs, rows, columns // per), jnp.bfloat16),
+            pltpu.VMEM(normed.shape, jnp.float32),
             dma((2, experts)),
             dma((2, experts)),
             dma((2, experts, per)),
@@ -160,16 +190,56 @@
             dma((3, experts)),
             dma((3, experts)),
             dma((3, experts)),
+            dma((3,)),
         ],
-        compiler_params=pltpu.CompilerParams(has_side_effects=True),
-    )(*blocks)
-    return tuple(out.reshape(experts, n_fs * rows, columns // per) for out in outs[:3])
+        compiler_params=pltpu.CompilerParams(has_side_effects=True, vmem_limit_bytes=60 * 1024 * 1024),
+    )(*blocks, normed, gates.T[:, :, None])
+    return tuple(out.reshape(experts, n_fs * rows, columns // per) for out in outs[:3]) + (outs[4],)
+
+
+def copy_kernel(*refs):
+    half = len(refs) // 2
+    for source, target in zip(refs[:half], refs[half:]):
+        target[...] = source[...]
+
+
+def copied(arrays):
+    experts, deep, unit = arrays[0].shape
+    block = pl.BlockSpec((1, deep, unit), lambda e: (e, 0, 0))
+    return pl.pallas_call(
+        copy_kernel,
+        grid=(experts,),
+        out_shape=tuple(jax.ShapeDtypeStruct(a.shape, a.dtype) for a in arrays),
+        in_specs=[block] * len(arrays),
+        out_specs=[block] * len(arrays),
+        cost_estimate=pl.CostEstimate(flops=0, bytes_accessed=4 * len(arrays) * arrays[0].size, transcendentals=0),
+        compiler_params=pltpu.CompilerParams(vmem_limit_bytes=40 * 1024 * 1024),
+    )(*arrays)
 
 
 def collective_exchange(blocks):
     regrouped = [lax.all_to_all(b, "tp", split_axis=0, concat_axis=2, tiled=True) for b in blocks]
     unit_split = [lax.all_to_all(b, "fs", split_axis=2, concat_axis=1, tiled=True) for b in regrouped]
     return tuple(lax.all_gather(b, "tp", axis=0, tiled=True) for b in unit_split)
+
+
+def expert_layer(normed, expert_gates, gate_serve, up_serve, down_serve):
+    gate_act = jnp.einsum("rd,edf->ref", normed, gate_serve, preferred_element_type=jnp.float32)
+    up_act = jnp.einsum("rd,edf->ref", normed, up_serve, preferred_element_type=jnp.float32)
+    hidden = (jax.nn.silu(gate_act) * up_act * expert_gates[:, :, None]).astype(jnp.bfloat16)
+    return jnp.einsum("ref,edf->rd", hidden, down_serve, preferred_element_type=jnp.float32).astype(jnp.bfloat16)
+
+
+def sum_parts(parts, n_fs):
+    if n_fs > 8:
+        parts = lax.all_to_all(parts, "fs", split_axis=0, concat_axis=0, tiled=True)
+        return jnp.sum(parts.astype(jnp.float32), axis=0)
+    f = lax.axis_index("fs")
+    got = [lax.dynamic_index_in_dim(parts, f, 0, keepdims=False)]
+    for j in range(1, n_fs):
+        mine = lax.dynamic_index_in_dim(parts, lax.rem(f + j, n_fs), 0, keepdims=False)
+        got.append(lax.ppermute(mine, "fs", [(i, (i + j) % n_fs) for i in range(n_fs)]))
+    return sum(g.astype(jnp.float32) for g in got)
 
 
 def local(tokens, norm_gain, gate_weight, up_weight, down_weight, expert_ids, expert_mix):
@@ -179,12 +249,6 @@
         (up_weight * norm_gain[None, :, None]).astype(jnp.bfloat16),
         down_weight.astype(jnp.bfloat16),
     )
-    rows, columns = blocks[0].shape[1:]
-    unit = columns * n_tp // n_fs
-    if n_tp == 4 and n_fs % n_tp == 0 and unit % 128 == 0 and rows % 16 == 0:
-        gate_serve, up_serve, down_serve = exchange(n_fs, n_tp, blocks)
-    else:
-        gate_serve, up_serve, down_serve = collective_exchange(blocks)
     width = tokens.shape[2]
     token_rows = tokens.reshape(-1, width).astype(jnp.float32)
     row_mean = jnp.mean(token_rows, axis=1, keepdims=True)
@@ -193,20 +257,23 @@
     normed = (centered * lax.rsqrt(variance + norm_eps)).astype(jnp.bfloat16)
     route_ids = expert_ids.reshape(-1, 2)
     route_mix = expert_mix.reshape(-1, 2)
-    expert_iota = jnp.arange(gate_serve.shape[0], dtype=jnp.int32)
+    expert_iota = jnp.arange(gate_weight.shape[0], dtype=jnp.int32)
     expert_gates = jnp.sum(
         (route_ids[:, :, None] == expert_iota[None, None, :]).astype(jnp.float32)
         * route_mix[:, :, None],
         axis=1,
     )
-    gate_act = jnp.einsum("rd,edf->ref", normed, gate_serve, preferred_element_type=jnp.float32)
-    up_act = jnp.einsum("rd,edf->ref", normed, up_serve, preferred_element_type=jnp.float32)
-    hidden = (jax.nn.silu(gate_act) * up_act * expert_gates[:, :, None]).astype(jnp.bfloat16)
+    rows, columns = blocks[0].shape[1:]
+    unit = columns * n_tp // n_fs
+    halves = token_rows.shape[0] % 32 == 0
+    if n_tp == 4 and n_fs % n_tp == 0 and unit % 128 == 0 and rows % 16 == 0 and halves:
+        gate_serve, up_serve, down_serve, partial = exchange(n_fs, n_tp, blocks, normed, expert_gates)
+        gate_serve, up_serve, down_serve = copied((gate_serve, up_serve, down_serve))
+    else:
+        gate_serve, up_serve, down_serve = collective_exchange(blocks)
+        partial = expert_layer(normed, expert_gates, gate_serve, up_serve, down_serve)
     own_rows = token_rows.shape[0] // n_fs
-    partial = jnp.einsum("ref,edf->rd", hidden, down_serve, preferred_element_type=jnp.float32)
-    parts = partial.astype(jnp.bfloat16).reshape(n_fs, own_rows, width)
-    parts = lax.all_to_all(parts, "fs", split_axis=0, concat_axis=0, tiled=True)
-    summed = jnp.sum(parts.astype(jnp.float32), axis=0)
+    summed = sum_parts(partial.reshape(n_fs, own_rows, width), n_fs)
     mixed = summed.astype(jnp.bfloat16).reshape(own_rows, 1, width)
     return (gate_serve, up_serve, down_serve, mixed)
 

time: 597 us -> 545 us (0.913)
  the two profiles are of different devices: /device:TPU:0 before, /device:TPU:29 now
where the time goes in v2:
time: 545 us
  Pallas kernels  467 us (86%)
  starting transfers between devices  37.5 us (7%)
  other arithmetic  25.8 us (5%)
  waiting for transfers between devices  9.34 us (2%)
    pallas_call x1, Pallas kernels, exchange(): pl.pallas_call(functools.partial(exchange_kernel, n_fs, n_tp), out_shape=...  435 us
    ppermute x7, starting transfers between devices, sum_parts(): lax.ppermute(mine, 'fs', [(i, (i + j) % n_fs) for i in range(n_fs)])  37.5 us
    pallas_call x1, Pallas kernels, copied(): pl.pallas_call(copy_kernel, grid=(experts,), out_shape=tuple((jax.ShapeDt...  32 us
    convert_element_type x1, other arithmetic, local(): (up_weight * norm_gain[None, :, None]).astype(jnp.bfloat16)  11.9 us
  transfers between devices with their start and end apart: 7, of which 2 were waited for; matrix products, arithmetic and copies ran while one was open for 0% of the time, Pallas kernels for 6%

profile of v2, /device:TPU:29, one launch (start us, length us, event | category | flops | bytes accessed | tf_op | source)
XLA Modules:
  0.0 544.9 jit_solution(10112904113059117795)
XLA Ops:
  0.6 0.0 copy-start
  0.7 0.0 copy-start.1
  0.7 2.5 convert_reduce_fusion
  3.2 3.6 fusion.3
  6.8 0.0 copy-done
  6.8 2.5 fusion.4.normed
  9.3 0.0 copy-done.1
  9.3 0.0 copy-start.2
  9.3 0.0 copy-start.3
  9.4 0.0 copy-start.4
  9.4 2.7 convert_element_type.51.down_in
  12.0 0.0 copy-done.2
  12.0 0.0 copy-done.3
  12.0 2.2 copy.16.gates
  14.3 0.0 copy-done.4
  14.3 11.9 %multiply_convert_fusion = (bf16[8,256,1024]{2,1,0:T(8,128)(2,1)}, bf16[8,256,1024]{2,1,0:T(8,128)(2,1)}) fusion(f32[8,256,1024]{2,1,0:T(8,128)} %param.10, f32[256]{0:T(256)S(1)} %copy-done.4, f32[8,256,1024]{2,1,0:T(8,128)} %param.9), kind=kLoop, calls=%fused_computation | loop fusion | flops 8388608 | bytes 25166848 | tf_op jit(solution)/shard_map/convert_element_type | solution.py:249
  26.2 435.2 %shard_map.102 = (bf16[8,8,256,512]{3,2,1,0:T(8,128)(2,1)}, bf16[8,8,256,512]{3,2,1,0:T(8,128)(2,1)}, bf16[8,8,256,512]{3,2,1,0:T(8,128)(2,1)}, bf16[2,8,256,1024]{3,2,1,0:T(8,128)(2,1)}, bf16[768,2048]{1,0:T(8,128)(2,1)}) custom-call(bf16[8,256,1024]{2,1,0:T(8,128)(2,1)} %get-tuple-element.26.gate_in, bf16[8,256,1024]{2,1,0:T(8,128)(2,1)} %get-tuple-element.25.up_in, ...), custom_call_target="tpu_custom_call" | custom-call | tf_op jit(solution)/shard_map/pallas_call | solution.py:178
  461.4 2.1 dynamic-slice_bitcast_fusion.6
  463.5 6.0 %collective-permute-start = (bf16[96,2048]{1,0:T(8,128)(2,1)S(1)}, bf16[96,2048]{1,0:T(8,128)(2,1)S(1)}, u32[]{:S(2)}, u32[]{:S(2)}) collective-permute-start(bf16[96,2048]{1,0:T(8,128)(2,1)S(1)} %get-tuple-element.18), channel_id=1, source_target_pairs={{0,4},{4,8},{8,12},{12,16},{16,20},{20,24},{24,28},{28,0},{1,5},{5... | collective-permute-start | bytes 1179656 | tf_op jit(solution)/shard_map/ppermute | solution.py:241
  469.4 0.0 collective-permute-start.1
  469.4 0.0 collective-permute-start.2
  469.4 2.4 collective-permute-start.3
  471.8 0.8 collective-permute-start.4
  472.7 5.5 %collective-permute-done = bf16[96,2048]{1,0:T(8,128)(2,1)S(1)} collective-permute-done((bf16[96,2048]{1,0:T(8,128)(2,1)S(1)}, bf16[96,2048]{1,0:T(8,128)(2,1)S(1)}, u32[]{:S(2)}, u32[]{:S(2)}) %collective-permute-start) | collective-permute-done | bytes 393248 | tf_op jit(solution)/shard_map/ppermute | solution.py:241
  478.2 0.0 collective-permute-start.5
  478.2 3.9 collective-permute-done.1
  482.0 28.3 %collective-permute-start.6 = (bf16[96,2048]{1,0:T(8,128)(2,1)S(1)}, bf16[96,2048]{1,0:T(8,128)(2,1)S(1)}, u32[]{:S(2)}, u32[]{:S(2)}) collective-permute-start(bf16[96,2048]{1,0:T(8,128)(2,1)S(1)} %get-tuple-element.19), channel_id=1, source_target_pairs={{0,28},{4,0},{8,4},{12,8},{16,12},{20,16},{24,20},{28,24},{1,29},{... | collective-permute-start | bytes 1179656 | tf_op jit(solution)/shard_map/ppermute | solution.py:241
  510.3 32.0 %shard_map.103 = (bf16[8,2048,512]{2,1,0:T(8,128)(2,1)}, bf16[8,2048,512]{2,1,0:T(8,128)(2,1)}, bf16[8,2048,512]{2,1,0:T(8,128)(2,1)}) custom-call(bf16[8,2048,512]{2,1,0:T(8,128)(2,1)} %bitcast.40, bf16[8,2048,512]{2,1,0:T(8,128)(2,1)} %bitcast.41, bf16[8,2048,512]{2,1,0:T(8,128)(2,1)} %bitcast.42), custom_call_target="tpu_custom_call" | custom-call | bytes 100663296 | tf_op jit(solution)/shard_map/pallas_call | solution.py:209
  542.3 0.0 collective-permute-done.2
  542.3 0.0 collective-permute-done.3
  542.3 0.0 collective-permute-done.4
  542.3 0.0 collective-permute-done.5
  542.3 0.0 collective-permute-done.6
  542.3 2.6 fusion.12
  (3 shorter events, 0.0 us)
Async XLA Ops:
  0.6 6.2 %copy-start = (bf16[768,1,2048]{2,0,1:T(8,128)(2,1)S(1)}, bf16[768,1,2048]{2,0,1:T(8,128)(2,1)}, u32[]{:S(2)}) copy-start(bf16[768,1,2048]{2,0,1:T(8,128)(2,1)} %param.7) | copy-start | bytes 9437188
  0.7 8.7 %copy-start.1 = (f32[8,256,1024]{2,1,0:T(8,128)S(1)}, f32[8,256,1024]{2,1,0:T(8,128)}, u32[]{:S(2)}) copy-start(f32[8,256,1024]{2,1,0:T(8,128)} %param.11) | copy-start | bytes 25165828
  9.3 2.7 copy-start.2
  9.3 2.7 copy-start.3
  9.4 4.9 copy-start.4
  463.5 14.7 %collective-permute-start = (bf16[96,2048]{1,0:T(8,128)(2,1)S(1)}, bf16[96,2048]{1,0:T(8,128)(2,1)S(1)}, u32[]{:S(2)}, u32[]{:S(2)}) collective-permute-start(bf16[96,2048]{1,0:T(8,128)(2,1)S(1)} %get-tuple-element.18), channel_id=1, source_target_pairs={{0,4},{4,8},{8,12},{12,16},{16,20},{20,24},{24,28},{28,0},{1,5},{5... | collective-permute-start | bytes 1179656 | tf_op jit(solution)/shard_map/ppermute | solution.py:241
  469.4 12.6 %collective-permute-start.1 = (bf16[96,2048]{1,0:T(8,128)(2,1)S(1)}, bf16[96,2048]{1,0:T(8,128)(2,1)S(1)}, u32[]{:S(2)}, u32[]{:S(2)}) collective-permute-start(bf16[96,2048]{1,0:T(8,128)(2,1)S(1)} %get-tuple-element.24), channel_id=1, source_target_pairs={{0,8},{4,12},{8,16},{12,20},{16,24},{20,28},{24,0},{28,4},{1,9},{5... | collective-permute-start | bytes 1179656 | tf_op jit(solution)/shard_map/ppermute | solution.py:241
  469.4 72.9 %collective-permute-start.2 = (bf16[96,2048]{1,0:T(8,128)(2,1)S(1)}, bf16[96,2048]{1,0:T(8,128)(2,1)}, u32[]{:S(2)}, u32[]{:S(2)}) collective-permute-start(bf16[96,2048]{1,0:T(8,128)(2,1)S(1)} %get-tuple-element.23), channel_id=1, source_target_pairs={{0,12},{4,16},{8,20},{12,24},{16,28},{20,0},{24,4},{28,8},{1,13},{... | collective-permute-start | bytes 1179656 | tf_op jit(solution)/shard_map/ppermute | solution.py:241
  469.4 72.9 %collective-permute-start.3 = (bf16[96,2048]{1,0:T(8,128)(2,1)S(1)}, bf16[96,2048]{1,0:T(8,128)(2,1)}, u32[]{:S(2)}, u32[]{:S(2)}) collective-permute-start(bf16[96,2048]{1,0:T(8,128)(2,1)S(1)} %get-tuple-element.22), channel_id=1, source_target_pairs={{0,16},{4,20},{8,24},{12,28},{16,0},{20,4},{24,8},{28,12},{1,17},{... | collective-permute-start | bytes 1179656 | tf_op jit(solution)/shard_map/ppermute | solution.py:241
  471.8 70.4 %collective-permute-start.4 = (bf16[96,2048]{1,0:T(8,128)(2,1)S(1)}, bf16[96,2048]{1,0:T(8,128)(2,1)}, u32[]{:S(2)}, u32[]{:S(2)}) collective-permute-start(bf16[96,2048]{1,0:T(8,128)(2,1)S(1)} %get-tuple-element.21), channel_id=1, source_target_pairs={{0,20},{4,24},{8,28},{12,0},{16,4},{20,8},{24,12},{28,16},{1,21},{... | collective-permute-start | bytes 1179656 | tf_op jit(solution)/shard_map/ppermute | solution.py:241
  478.2 64.1 %collective-permute-start.5 = (bf16[96,2048]{1,0:T(8,128)(2,1)S(1)}, bf16[96,2048]{1,0:T(8,128)(2,1)S(1)}, u32[]{:S(2)}, u32[]{:S(2)}) collective-permute-start(bf16[96,2048]{1,0:T(8,128)(2,1)S(1)} %get-tuple-element.20), channel_id=1, source_target_pairs={{0,24},{4,28},{8,0},{12,4},{16,8},{20,12},{24,16},{28,20},{1,25},{... | collective-permute-start | bytes 1179656 | tf_op jit(solution)/shard_map/ppermute | solution.py:241
  482.0 60.3 %collective-permute-start.6 = (bf16[96,2048]{1,0:T(8,128)(2,1)S(1)}, bf16[96,2048]{1,0:T(8,128)(2,1)S(1)}, u32[]{:S(2)}, u32[]{:S(2)}) collective-permute-start(bf16[96,2048]{1,0:T(8,128)(2,1)S(1)} %get-tuple-element.19), channel_id=1, source_target_pairs={{0,28},{4,0},{8,4},{12,8},{16,12},{20,16},{24,20},{28,24},{1,29},{... | collective-permute-start | bytes 1179656 | tf_op jit(solution)/shard_map/ppermute | solution.py:241

commit v3 on v2

--- a/solution.py
+++ b/solution.py
@@ -96,9 +96,9 @@
                 for h in range(per):
                     relayed(k, s - 1, h).start()
 
-        @pl.when((s >= 2) & (s < experts + 2))
-        def _():
-            e = s - 2
+        @pl.when((s >= 3) & (s < experts + 3))
+        def _():
+            e = s - 3
 
             @pl.when(near)
             def _():
@@ -116,9 +116,9 @@
                 landed(1, e)
                 to_mate(1, e).start()
 
-        @pl.when(s >= 3)
-        def _():
-            e = s - 3
+        @pl.when(s >= 4)
+        def _():
+            e = s - 4
 
             @pl.when(near)
             def _():
@@ -139,7 +139,7 @@
 
         return carry
 
-    lax.fori_loop(0, experts + 3, step, 0)
+    lax.fori_loop(0, experts + 4, step, 0)
     partial[...] = total[...].astype(jnp.bfloat16)
 
     def drain(e, carry):

time: 545 us -> 540 us (level)
  starting transfers between devices: 37.5 us -> 62.7 us
  Pallas kernels: 467 us -> 446 us
  waiting for transfers between devices: 9.34 us -> 0.02 us
    ppermute x7, starting transfers between devices: 37.5 us -> 62.7 us  [sum_parts(): lax.ppermute(mine, 'fs', [(i, (i + j) % n_fs) for i in range(n_fs)])]
    pallas_call x1, Pallas kernels: 435 us -> 414 us  [exchange(): pl.pallas_call(functools.partial(exchange_kernel, n_fs, n_tp), out_shape=...]
    ppermute x7, waiting for transfers between devices: 9.34 us -> 0.02 us  [sum_parts(): lax.ppermute(mine, 'fs', [(i, (i + j) % n_fs) for i in range(n_fs)])]
  transfers between devices with their start and end apart: 7 -> 7, of which waited for: 2 -> 0; matrix products, arithmetic and copies ran while one was open for 0% -> 0% of each run, Pallas kernels for 6% -> 6%
where the time goes in v3:
time: 540 us
  Pallas kernels  446 us (83%)
  starting transfers between devices  62.7 us (12%)
  other arithmetic  25.8 us (5%)
    pallas_call x1, Pallas kernels, exchange(): pl.pallas_call(functools.partial(exchange_kernel, n_fs, n_tp), out_shape=...  414 us
    ppermute x7, starting transfers between devices, sum_parts(): lax.ppermute(mine, 'fs', [(i, (i + j) % n_fs) for i in range(n_fs)])  62.7 us
    pallas_call x1, Pallas kernels, copied(): pl.pallas_call(copy_kernel, grid=(experts,), out_shape=tuple((jax.ShapeDt...  32 us
    convert_element_type x1, other arithmetic, local(): (up_weight * norm_gain[None, :, None]).astype(jnp.bfloat16)  11.9 us
  transfers between devices with their start and end apart: 7, of which 0 were waited for; matrix products, arithmetic and copies ran while one was open for 0% of the time, Pallas kernels for 6%

profile of v3, /device:TPU:29, one launch (start us, length us, event | category | flops | bytes accessed | tf_op | source)
XLA Modules:
  0.0 539.8 jit_solution(9326292858972699957)
XLA Ops:
  0.6 0.0 copy-start
  0.7 0.0 copy-start.1
  0.7 2.5 convert_reduce_fusion
  3.2 3.6 fusion.3
  6.8 0.0 copy-done
  6.8 2.5 fusion.4.normed
  9.3 0.0 copy-done.1
  9.3 0.0 copy-start.2
  9.3 0.0 copy-start.3
  9.4 0.0 copy-start.4
  9.4 2.7 convert_element_type.51.down_in
  12.0 0.0 copy-done.2
  12.0 0.0 copy-done.3
  12.0 2.2 copy.16.gates
  14.3 0.0 copy-done.4
  14.3 11.9 %multiply_convert_fusion = (bf16[8,256,1024]{2,1,0:T(8,128)(2,1)}, bf16[8,256,1024]{2,1,0:T(8,128)(2,1)}) fusion(f32[8,256,1024]{2,1,0:T(8,128)} %param.10, f32[256]{0:T(256)S(1)} %copy-done.4, f32[8,256,1024]{2,1,0:T(8,128)} %param.9), kind=kLoop, calls=%fused_computation | loop fusion | flops 8388608 | bytes 25166848 | tf_op jit(solution)/shard_map/convert_element_type | solution.py:249
  26.2 414.2 %shard_map.102 = (bf16[8,8,256,512]{3,2,1,0:T(8,128)(2,1)}, bf16[8,8,256,512]{3,2,1,0:T(8,128)(2,1)}, bf16[8,8,256,512]{3,2,1,0:T(8,128)(2,1)}, bf16[2,8,256,1024]{3,2,1,0:T(8,128)(2,1)}, bf16[768,2048]{1,0:T(8,128)(2,1)}) custom-call(bf16[8,256,1024]{2,1,0:T(8,128)(2,1)} %get-tuple-element.26.gate_in, bf16[8,256,1024]{2,1,0:T(8,128)(2,1)} %get-tuple-element.25.up_in, ...), custom_call_target="tpu_custom_call" | custom-call | tf_op jit(solution)/shard_map/pallas_call | solution.py:178
  440.4 2.1 dynamic-slice_bitcast_fusion.6
  442.5 6.0 %collective-permute-start = (bf16[96,2048]{1,0:T(8,128)(2,1)S(1)}, bf16[96,2048]{1,0:T(8,128)(2,1)S(1)}, u32[]{:S(2)}, u32[]{:S(2)}) collective-permute-start(bf16[96,2048]{1,0:T(8,128)(2,1)S(1)} %get-tuple-element.18), channel_id=1, source_target_pairs={{0,4},{4,8},{8,12},{12,16},{16,20},{20,24},{24,28},{28,0},{1,5},{5... | collective-permute-start | bytes 1179656 | tf_op jit(solution)/shard_map/ppermute | solution.py:241
  448.4 1.8 collective-permute-start.1
  450.2 4.5 collective-permute-start.2
  454.7 0.0 collective-permute-start.3
  454.7 2.3 collective-permute-start.4
  457.0 0.0 collective-permute-done
  457.0 6.1 %collective-permute-start.5 = (bf16[96,2048]{1,0:T(8,128)(2,1)S(1)}, bf16[96,2048]{1,0:T(8,128)(2,1)S(1)}, u32[]{:S(2)}, u32[]{:S(2)}) collective-permute-start(bf16[96,2048]{1,0:T(8,128)(2,1)S(1)} %get-tuple-element.20), channel_id=1, source_target_pairs={{0,24},{4,28},{8,0},{12,4},{16,8},{20,12},{24,16},{28,20},{1,25},{... | collective-permute-start | bytes 1179656 | tf_op jit(solution)/shard_map/ppermute | solution.py:241
  463.1 0.0 collective-permute-done.1
  463.1 42.1 %collective-permute-start.6 = (bf16[96,2048]{1,0:T(8,128)(2,1)S(1)}, bf16[96,2048]{1,0:T(8,128)(2,1)S(1)}, u32[]{:S(2)}, u32[]{:S(2)}) collective-permute-start(bf16[96,2048]{1,0:T(8,128)(2,1)S(1)} %get-tuple-element.19), channel_id=1, source_target_pairs={{0,28},{4,0},{8,4},{12,8},{16,12},{20,16},{24,20},{28,24},{1,29},{... | collective-permute-start | bytes 1179656 | tf_op jit(solution)/shard_map/ppermute | solution.py:241
  505.2 32.0 %shard_map.103 = (bf16[8,2048,512]{2,1,0:T(8,128)(2,1)}, bf16[8,2048,512]{2,1,0:T(8,128)(2,1)}, bf16[8,2048,512]{2,1,0:T(8,128)(2,1)}) custom-call(bf16[8,2048,512]{2,1,0:T(8,128)(2,1)} %bitcast.40, bf16[8,2048,512]{2,1,0:T(8,128)(2,1)} %bitcast.41, bf16[8,2048,512]{2,1,0:T(8,128)(2,1)} %bitcast.42), custom_call_target="tpu_custom_call" | custom-call | bytes 100663296 | tf_op jit(solution)/shard_map/pallas_call | solution.py:209
  537.2 0.0 collective-permute-done.2
  537.2 0.0 collective-permute-done.3
  537.2 0.0 collective-permute-done.4
  537.2 0.0 collective-permute-done.5
  537.2 0.0 collective-permute-done.6
  537.2 2.6 fusion.12
  (3 shorter events, 0.0 us)
Async XLA Ops:
  0.6 6.2 %copy-start = (bf16[768,1,2048]{2,0,1:T(8,128)(2,1)S(1)}, bf16[768,1,2048]{2,0,1:T(8,128)(2,1)}, u32[]{:S(2)}) copy-start(bf16[768,1,2048]{2,0,1:T(8,128)(2,1)} %param.7) | copy-start | bytes 9437188
  0.7 8.7 %copy-start.1 = (f32[8,256,1024]{2,1,0:T(8,128)S(1)}, f32[8,256,1024]{2,1,0:T(8,128)}, u32[]{:S(2)}) copy-start(f32[8,256,1024]{2,1,0:T(8,128)} %param.11) | copy-start | bytes 25165828
  9.3 2.7 copy-start.2
  9.3 2.7 copy-start.3
  9.4 4.9 copy-start.4
  442.5 14.5 %collective-permute-start = (bf16[96,2048]{1,0:T(8,128)(2,1)S(1)}, bf16[96,2048]{1,0:T(8,128)(2,1)S(1)}, u32[]{:S(2)}, u32[]{:S(2)}) collective-permute-start(bf16[96,2048]{1,0:T(8,128)(2,1)S(1)} %get-tuple-element.18), channel_id=1, source_target_pairs={{0,4},{4,8},{8,12},{12,16},{16,20},{20,24},{24,28},{28,0},{1,5},{5... | collective-permute-start | bytes 1179656 | tf_op jit(solution)/shard_map/ppermute | solution.py:241
  448.4 14.7 %collective-permute-start.1 = (bf16[96,2048]{1,0:T(8,128)(2,1)S(1)}, bf16[96,2048]{1,0:T(8,128)(2,1)S(1)}, u32[]{:S(2)}, u32[]{:S(2)}) collective-permute-start(bf16[96,2048]{1,0:T(8,128)(2,1)S(1)} %get-tuple-element.24), channel_id=1, source_target_pairs={{0,8},{4,12},{8,16},{12,20},{16,24},{20,28},{24,0},{28,4},{1,9},{5... | collective-permute-start | bytes 1179656 | tf_op jit(solution)/shard_map/ppermute | solution.py:241
  450.2 87.0 %collective-permute-start.2 = (bf16[96,2048]{1,0:T(8,128)(2,1)S(1)}, bf16[96,2048]{1,0:T(8,128)(2,1)}, u32[]{:S(2)}, u32[]{:S(2)}) collective-permute-start(bf16[96,2048]{1,0:T(8,128)(2,1)S(1)} %get-tuple-element.23), channel_id=1, source_target_pairs={{0,12},{4,16},{8,20},{12,24},{16,28},{20,0},{24,4},{28,8},{1,13},{... | collective-permute-start | bytes 1179656 | tf_op jit(solution)/shard_map/ppermute | solution.py:241
  454.7 82.5 %collective-permute-start.3 = (bf16[96,2048]{1,0:T(8,128)(2,1)S(1)}, bf16[96,2048]{1,0:T(8,128)(2,1)}, u32[]{:S(2)}, u32[]{:S(2)}) collective-permute-start(bf16[96,2048]{1,0:T(8,128)(2,1)S(1)} %get-tuple-element.22), channel_id=1, source_target_pairs={{0,16},{4,20},{8,24},{12,28},{16,0},{20,4},{24,8},{28,12},{1,17},{... | collective-permute-start | bytes 1179656 | tf_op jit(solution)/shard_map/ppermute | solution.py:241
  454.7 82.6 %collective-permute-start.4 = (bf16[96,2048]{1,0:T(8,128)(2,1)S(1)}, bf16[96,2048]{1,0:T(8,128)(2,1)}, u32[]{:S(2)}, u32[]{:S(2)}) collective-permute-start(bf16[96,2048]{1,0:T(8,128)(2,1)S(1)} %get-tuple-element.21), channel_id=1, source_target_pairs={{0,20},{4,24},{8,28},{12,0},{16,4},{20,8},{24,12},{28,16},{1,21},{... | collective-permute-start | bytes 1179656 | tf_op jit(solution)/shard_map/ppermute | solution.py:241
  457.0 80.3 %collective-permute-start.5 = (bf16[96,2048]{1,0:T(8,128)(2,1)S(1)}, bf16[96,2048]{1,0:T(8,128)(2,1)S(1)}, u32[]{:S(2)}, u32[]{:S(2)}) collective-permute-start(bf16[96,2048]{1,0:T(8,128)(2,1)S(1)} %get-tuple-element.20), channel_id=1, source_target_pairs={{0,24},{4,28},{8,0},{12,4},{16,8},{20,12},{24,16},{28,20},{1,25},{... | collective-permute-start | bytes 1179656 | tf_op jit(solution)/shard_map/ppermute | solution.py:241
  463.1 74.2 %collective-permute-start.6 = (bf16[96,2048]{1,0:T(8,128)(2,1)S(1)}, bf16[96,2048]{1,0:T(8,128)(2,1)S(1)}, u32[]{:S(2)}, u32[]{:S(2)}) collective-permute-start(bf16[96,2048]{1,0:T(8,128)(2,1)S(1)} %get-tuple-element.19), channel_id=1, source_target_pairs={{0,28},{4,0},{8,4},{12,8},{16,12},{20,16},{24,20},{28,24},{1,29},{... | collective-permute-start | bytes 1179656 | tf_op jit(solution)/shard_map/ppermute | solution.py:241
